TPU v7x, 32 devices: a whole 2x2x4 slice. The times are simulated.
32 devices in a mesh: fs: 4 (over z), rep: 4 (over y, x), tp: 2 (over core).
Axes of the slice: x: 2, y: 2, z: 4, core: 2. Of those that a mesh axis runs over, the one named last changes fastest.
Arguments:
- input_act: bfloat16 [12288, 2048], P(('fs', 'rep')), may hold values from -6 to 6
- query_cot: bfloat16 [12288, 1024], P(('fs', 'rep'), 'tp'), may hold values from -6 to 6
- out_cot: bfloat16 [12288, 2048], P(('fs', 'rep')), may hold values from -6 to 6
- attn_out: bfloat16 [12288, 1024], P(('fs', 'rep'), 'tp'), may hold values from -6 to 6
- query_w: float32 [2048, 1024], P('fs', 'tp'), may hold values from -0.125 to 0.125
- out_w: float32 [1024, 2048], P('tp', 'fs'), may hold values from -0.1875 to 0.1875
- query_factor: bfloat16 [2048, 512], P('fs'), may hold values from -0.125 to 0.125
- out_factor: bfloat16 [2048, 512], P('fs'), may hold values from -0.125 to 0.125
- first_q: float32 [512, 1024], P('fs', 'tp'), may hold values from -6 to 6
- second_q: float32 [512, 1024], P('fs', 'tp'), may hold values from 0.075 to 120
- first_o: float32 [512, 1024], P('fs', 'tp'), may hold values from -6 to 6
- second_o: float32 [512, 1024], P('fs', 'tp'), may hold values from 0.075 to 120
Outputs:
- new_query_w: float32 [2048, 1024], P('fs', 'tp')
- new_out_w: float32 [1024, 2048], P('tp', 'fs')
- query_step: float32 [2048, 1024], P('fs', 'tp')
- out_step: float32 [1024, 2048], P('tp', 'fs')
- new_first_q: float32 [512, 1024], P('fs', 'tp')
- new_second_q: float32 [512, 1024], P('fs', 'tp')
- new_first_o: float32 [512, 1024], P('fs', 'tp')
- new_second_o: float32 [512, 1024], P('fs', 'tp')
- query_copy: bfloat16 [2048, 1024], P(None, 'tp')
- out_copy: bfloat16 [1024, 2048], P('tp')
All inputs are finite; a program needn't handle non-finite values.
Results may differ from a plain program's by a relative error of at most 0.0085.
Values may be sent and summed in bfloat16 or wider, within the bound.
A program may use at most 64 MiB of HBM per device.

v0:
```python
import math
import jax
import jax.numpy as jnp
from jax import lax
from jax.sharding import PartitionSpec as P

RANK = 512
HQ = 1024


def contract_rows(left_side, right_side):
    return lax.dot_general(
        left_side, right_side, (((0,), (0,)), ((), ())), preferred_element_type=jnp.float32
    )


def contract_exact(left_side, right_side):
    return lax.dot_general(
        left_side.astype(jnp.float32),
        right_side,
        (((0,), (0,)), ((), ())),
        precision=lax.Precision.HIGHEST,
        preferred_element_type=jnp.float32,
    )


def exact_dot(left_side, right_side):
    return jnp.dot(
        left_side, right_side, precision=lax.Precision.HIGHEST, preferred_element_type=jnp.float32
    )


def body(
    input_act,
    query_cot,
    out_cot,
    attn_out,
    query_w,
    out_w,
    query_factor,
    out_factor,
    first_q,
    second_q,
    first_o,
    second_o,
):
    heads_local = query_cot.shape[1]
    token_total = input_act.shape[0] * lax.axis_size("fs") * lax.axis_size("rep")
    scale_tokens = 1.0 / math.sqrt(token_total)
    gradient = lax.psum_scatter(
        jnp.concatenate(
            [contract_rows(input_act, query_cot), contract_rows(out_cot, attn_out)], axis=1
        ).astype(jnp.bfloat16),
        "fs",
        scatter_dimension=0,
        tiled=True,
    ).astype(jnp.float32)
    partial_value = jnp.concatenate(
        [
            contract_exact(query_factor, gradient[:, :heads_local]),
            contract_exact(out_factor, gradient[:, heads_local:]),
        ],
        axis=1,
    )
    projected = lax.psum_scatter(
        partial_value.astype(jnp.bfloat16), "fs", scatter_dimension=0, tiled=True
    ).astype(jnp.float32)
    projected = lax.psum(projected.astype(jnp.bfloat16), "rep").astype(jnp.float32) * scale_tokens
    proj_q = projected[:, :heads_local]
    proj_o = projected[:, heads_local:]
    new_first_q = 0.8 * first_q + 0.2 * proj_q
    new_second_q = 0.9 * second_q + 0.1 * proj_q * proj_q
    new_first_o = 0.8 * first_o + 0.2 * proj_o
    new_second_o = 0.9 * second_o + 0.1 * proj_o * proj_o
    dir_q = new_first_q / jnp.sqrt(new_second_q)
    dir_o = new_first_o / jnp.sqrt(new_second_o)
    local_squares = jnp.sum(dir_q * dir_q) + jnp.sum(dir_o * dir_o)
    total_squares = lax.psum(local_squares, ("fs", "tp"))
    norm_scale = jnp.sqrt(total_squares / (2 * RANK * HQ) + 1e-06)
    whole_dir_q, whole_dir_o = (
        lax.all_gather(dir_q, "fs", axis=0, tiled=True),
        lax.all_gather(dir_o, "fs", axis=0, tiled=True),
    )
    query_step = exact_dot(query_factor.astype(jnp.float32), whole_dir_q) / norm_scale
    out_step = (exact_dot(out_factor.astype(jnp.float32), whole_dir_o) / norm_scale).T
    new_query_w = query_w - 0.01 * query_step
    new_out_w = out_w - 0.01 * out_step
    query_copy = lax.all_gather(new_query_w.astype(jnp.bfloat16), "fs", axis=0, tiled=True)
    out_copy = lax.all_gather(new_out_w.astype(jnp.bfloat16), "fs", axis=1, tiled=True)
    return (
        new_query_w,
        new_out_w,
        query_step,
        out_step,
        new_first_q,
        new_second_q,
        new_first_o,
        new_second_o,
        query_copy,
        out_copy,
    )


def solution(mesh):
    return jax.shard_map(
        body,
        mesh=mesh,
        in_specs=(
            P(("fs", "rep"), None),
            P(("fs", "rep"), "tp"),
            P(("fs", "rep"), None),
            P(("fs", "rep"), "tp"),
            P("fs", "tp"),
            P("tp", "fs"),
            P("fs", None),
            P("fs", None),
            P("fs", "tp"),
            P("fs", "tp"),
            P("fs", "tp"),
            P("fs", "tp"),
        ),
        out_specs=(
            P("fs", "tp"),
            P("tp", "fs"),
            P("fs", "tp"),
            P("tp", "fs"),
            P("fs", "tp"),
            P("fs", "tp"),
            P("fs", "tp"),
            P("fs", "tp"),
            P(None, "tp"),
            P("tp", None),
        ),
        check_vma=False,
    )
```

profile of v0, /device:TPU:0, one launch (start us, length us, event | category | flops | bytes accessed | tf_op | source)
XLA Modules:
  0.0 343.3 jit_solution(11248011831809214401)
XLA Ops:
  7.2 1.8 copy-done
  9.1 3.1 convolution_convert_fusion.1
  12.2 1.9 convolution_convert_fusion
  14.1 2.5 pad_maximum_fusion
  16.8 79.6 %reduce-scatter.5.cloned.1.call-done = bf16[512,1024]{0,1:T(8,128)(2,1)} async-done(((bf16[2048,1024]{0,1:T(8,128)(2,1)}), bf16[512,1024]{0,1:T(8,128)(2,1)}) %reduce-scatter.5.cloned.1.call-update) | async-done | bytes 1048592 | tf_op jit(solution)/shard_map/reduce_scatter | solution.py:50
  98.0 1.6 fusion.1
  100.7 2.3 copy.59
  103.0 27.9 %reduce-scatter.7.cloned.1.call-done = bf16[128,1024]{1,0:T(8,128)(2,1)} async-done(((bf16[512,1024]{1,0:T(8,128)(2,1)}), bf16[128,1024]{1,0:T(8,128)(2,1)}) %reduce-scatter.7.cloned.1.call-update) | async-done | bytes 262160
  130.9 1.8 copy.60
  133.7 1.8 copy.41
  135.4 1.8 copy.42
  137.2 1.8 copy.43
  139.0 37.0 %all-reduce.2.cloned.1.call-done = bf16[128,1024]{0,1:T(8,128)(2,1)} async-done(((bf16[128,1024]{0,1:T(8,128)(2,1)}), bf16[128,1024]{0,1:T(8,128)(2,1)}) %all-reduce.2.cloned.1.call-update) | async-done | bytes 262160 | tf_op jit(solution)/shard_map/psum | solution.py:68
  177.0 2.9 multiply_reduce_fusion
  181.9 2.5 copy.45
  184.4 16.9 %psum.15 = f32[]{:T(128)} all-reduce(f32[]{:T(128)S(6)} %add.30), channel_id=1, replica_groups=mesh['fs'=4,'rep'=4,'tp'=2] {'fs','tp'}, use_global_device_ids=true, to_apply=%region_5.0 | all-reduce | flops 1 | bytes 8 | tf_op jit(solution)/shard_map/psum | solution.py:78
  202.0 8.3 %all-gather.5.cloned.1.call-done = f32[512,512]{0,1:T(8,128)} async-done(((f32[128,512]{0,1:T(8,128)}), f32[512,512]{0,1:T(8,128)}) %all-gather.5.cloned.1.call-update) | async-done | bytes 1048592 | tf_op jit(solution)/shard_map/all_gather | solution.py:81
  210.3 4.2 %fusion.8 = (bf16[512,512]{0,1:T(8,128)(2,1)}, f32[512,512]{0,1:T(8,128)}, f32[512,512]{0,1:T(8,128)}) fusion(f32[512,512]{0,1:T(8,128)} %copy.45, f32[]{:T(128)S(6)} %sqrt.11, f32[512,512]{0,1:T(8,128)} %all-gather.5.cloned.1.call-done, bf16[512,512]{1,0:T(8,128)(2,1)} %param.18), kind=kOutput, calls=%fused_computation.27 | convolution fusion | flops 1611661312 | bytes 5242884 | tf_op jit(solution)/shard_map/dot_general | solution.py:28
  214.6 2.5 copy.47
  217.1 23.4 %all-gather.7.cloned.1.call-done = f32[512,512]{0,1:T(8,128)} async-done(((f32[128,512]{0,1:T(8,128)}), f32[512,512]{0,1:T(8,128)}) %all-gather.7.cloned.1.call-update) | async-done | bytes 1048592 | tf_op jit(solution)/shard_map/all_gather | solution.py:82
  240.5 4.3 %fusion.7 = (bf16[512,512]{0,1:T(8,128)(2,1)}, f32[512,512]{0,1:T(8,128)}, f32[512,512]{0,1:T(8,128)}) fusion(f32[512,512]{0,1:T(8,128)} %copy.47, f32[]{:T(128)S(6)} %sqrt.11, f32[512,512]{0,1:T(8,128)} %all-gather.7.cloned.1.call-done, bf16[512,512]{1,0:T(8,128)(2,1)} %param.19), kind=kOutput, calls=%fused_computation.26 | convolution fusion | flops 1611661312 | bytes 5242884 | tf_op jit(solution)/shard_map/dot_general | solution.py:28
  244.9 1.8 copy.55
  246.6 1.8 copy.54
  248.4 1.8 copy.53
  251.1 2.5 copy.49
  253.6 2.5 copy.51
  256.1 2.5 copy.48
  258.7 2.5 copy.50
  261.2 25.3 %all-gather.9.cloned.1.call-done = bf16[2048,512]{0,1:T(8,128)(2,1)} async-done(((bf16[512,512]{0,1:T(8,128)(2,1)}), bf16[2048,512]{0,1:T(8,128)(2,1)}) %all-gather.9.cloned.1.call-update) | async-done | bytes 2097168 | tf_op jit(solution)/shard_map/all_gather | solution.py:88
  286.5 3.9 %copy.56 = bf16[2048,512]{1,0:T(8,128)(2,1)} copy(bf16[2048,512]{0,1:T(8,128)(2,1)} %all-gather.9.cloned.1.call-done) | data formatting | bytes 4194304
  290.4 42.1 %all-gather.11.cloned.1.call-done = bf16[512,2048]{0,1:T(8,128)(2,1)} async-done(((bf16[512,512]{0,1:T(8,128)(2,1)}), bf16[512,2048]{0,1:T(8,128)(2,1)}) %all-gather.11.cloned.1.call-update) | async-done | bytes 2097168 | tf_op jit(solution)/shard_map/all_gather | solution.py:89
  332.6 3.9 %copy.57 = bf16[512,2048]{1,0:T(8,128)(2,1)} copy(bf16[512,2048]{0,1:T(8,128)(2,1)} %all-gather.11.cloned.1.call-done) | data formatting | bytes 4194304
  (26 shorter events, 6.3 us)
Async XLA Ops:
  7.2 1.9 copy-start
  7.2 89.2 %reduce-scatter.5.cloned.1.call-start = ((), (), s32[]{:S(2)}) async-start(), calls=%async_computation.2 | async-start | bytes 5242880 | tf_op jit(solution)/shard_map/reduce_scatter | solution.py:50
  9.1 3.1 copy-start.2
  9.1 3.1 copy-start.3
  16.7 114.2 %reduce-scatter.7.cloned.1.call-start = ((), (), s32[]{:S(2)}) async-start(), calls=%async_computation.8 | async-start | bytes 1310720
  99.7 33.2 %copy-start.1 = (f32[128,512]{1,0:T(8,128)S(1)}, f32[128,512]{1,0:T(8,128)}, u32[]{:S(2)}) copy-start(f32[128,512]{1,0:T(8,128)} %param.20) | copy-start | bytes 786436
  103.0 73.0 %all-reduce.2.cloned.1.call-start = ((), (), s32[]{:S(2)}) async-start(), calls=%async_computation.3 | async-start | bytes 524288 | tf_op jit(solution)/shard_map/psum | solution.py:68
  132.8 77.5 %all-gather.5.cloned.1.call-start = ((), (), s32[]{:S(2)}) async-start(), calls=%async_computation.4 | async-start | bytes 1310720 | tf_op jit(solution)/shard_map/all_gather | solution.py:81
  179.9 60.6 %all-gather.7.cloned.1.call-start = ((), (), s32[]{:S(2)}) async-start(), calls=%async_computation.5 | async-start | bytes 1310720 | tf_op jit(solution)/shard_map/all_gather | solution.py:82
  180.5 106.0 %all-gather.9.cloned.1.call-start = ((), (), s32[]{:S(2)}) async-start(), calls=%async_computation.6 | async-start | bytes 2621440 | tf_op jit(solution)/shard_map/all_gather | solution.py:88
  214.6 118.0 %all-gather.11.cloned.1.call-start = ((), (), s32[]{:S(2)}) async-start(), calls=%async_computation.7 | async-start | bytes 2621440 | tf_op jit(solution)/shard_map/all_gather | solution.py:89
Sparse Core Ops, SparseCore 0:
  16.8 79.5 reduce-scatter.4
  103.1 27.7 reduce-scatter.6
  134.4 41.5 all-reduce.1
  180.1 30.1 all-gather.4
  212.3 28.2 all-gather.6
  242.5 43.9 all-gather.8
  288.1 44.4 all-gather.10
where the time goes:
time: 344 us; the launch traced here: 343 us
  waiting for transfers between devices  244 us (71%)
  local copies, waits for them, and re-layouts  41.3 us (12%)
  blocking collectives  16.9 us (5%)
  matrix products  16.8 us (5%)
  between operations  16.2 us (5%)
  other arithmetic  7.46 us (2%)
    reduce_scatter x1, waiting for transfers between devices, body(): lax.psum_scatter(jnp.concatenate([contract_rows(input_act, query_cot), co...  79.6 us
    all_gather x1, waiting for transfers between devices, body(): lax.all_gather(new_out_w.astype(jnp.bfloat16), 'fs', axis=1, tiled=True)  42.1 us
    unnamed x26, local copies, waits for them, and re-layouts  41.3 us
    psum x1, waiting for transfers between devices, body(): lax.psum(projected.astype(jnp.bfloat16), 'rep').astype(jnp.float32)  37 us
    unnamed x8, waiting for transfers between devices  28.5 us
    all_gather x1, waiting for transfers between devices, body(): lax.all_gather(new_query_w.astype(jnp.bfloat16), 'fs', axis=0, tiled=True)  25.3 us
    all_gather x1, waiting for transfers between devices, body(): lax.all_gather(dir_o, 'fs', axis=0, tiled=True)  23.4 us
    psum x1, blocking collectives, body(): total_squares = lax.psum(local_squares, ('fs', 'tp'))  16.9 us
  transfers between devices with their start and end apart: 7, of which 7 were waited for; matrix products, arithmetic and copies ran while one was open for 12% of the time, Pallas kernels for 0%

commit v1 on v0

--- a/solution.py
+++ b/solution.py
@@ -65,7 +65,10 @@
     projected = lax.psum_scatter(
         partial_value.astype(jnp.bfloat16), "fs", scatter_dimension=0, tiled=True
     ).astype(jnp.float32)
-    projected = lax.psum(projected.astype(jnp.bfloat16), "rep").astype(jnp.float32) * scale_tokens
+    projected = (
+        jnp.sum(lax.all_gather(projected.astype(jnp.bfloat16), "rep"), axis=0).astype(jnp.float32)
+        * scale_tokens
+    )
     proj_q = projected[:, :heads_local]
     proj_o = projected[:, heads_local:]
     new_first_q = 0.8 * first_q + 0.2 * proj_q

time: 344 us -> 330 us (0.959)
  waiting for transfers between devices: 244 us -> 226 us
    psum x1 -> x0, waiting for transfers between devices: 37 us -> none  [body(): lax.psum(projected.astype(jnp.bfloat16), 'rep').astype(jnp.float32)]
    all_gather x0 -> x1, waiting for transfers between devices: none -> 19.2 us  [body(): lax.all_gather(projected.astype(jnp.bfloat16), 'rep')]
where the time goes in v1:
time: 330 us; the launch traced here: 329 us
  waiting for transfers between devices  226 us (68%)
  local copies, waits for them, and re-layouts  43.5 us (13%)
  blocking collectives  17.3 us (5%)
  matrix products  16.8 us (5%)
  between operations  16.2 us (5%)
  other arithmetic  9.01 us (3%)
    reduce_scatter x1, waiting for transfers between devices, body(): lax.psum_scatter(jnp.concatenate([contract_rows(input_act, query_cot), co...  79.6 us
    all_gather x1, waiting for transfers between devices, body(): lax.all_gather(new_out_w.astype(jnp.bfloat16), 'fs', axis=1, tiled=True)  42.1 us
    unnamed x26, local copies, waits for them, and re-layouts  41.3 us
    unnamed x8, waiting for transfers between devices  28.5 us
    all_gather x1, waiting for transfers between devices, body(): lax.all_gather(new_query_w.astype(jnp.bfloat16), 'fs', axis=0, tiled=True)  25.3 us
    all_gather x1, waiting for transfers between devices, body(): lax.all_gather(dir_o, 'fs', axis=0, tiled=True)  23.2 us
    all_gather x1, waiting for transfers between devices, body(): lax.all_gather(projected.astype(jnp.bfloat16), 'rep')  19.2 us
    psum x1, blocking collectives, body(): total_squares = lax.psum(local_squares, ('fs', 'tp'))  17.3 us
  transfers between devices with their start and end apart: 7, of which 7 were waited for; matrix products, arithmetic and copies ran while one was open for 12% of the time, Pallas kernels for 0%

profile of v1, /device:TPU:0, one launch (start us, length us, event | category | flops | bytes accessed | tf_op | source)
XLA Modules:
  0.0 329.3 jit_solution(9477046699237755518)
XLA Ops:
  7.2 1.8 copy-done
  9.1 3.1 convolution_convert_fusion.1
  12.2 1.9 convolution_convert_fusion
  14.1 2.5 pad_maximum_fusion
  16.8 79.6 %reduce-scatter.5.cloned.1.call-done = bf16[512,1024]{0,1:T(8,128)(2,1)} async-done(((bf16[2048,1024]{0,1:T(8,128)(2,1)}), bf16[512,1024]{0,1:T(8,128)(2,1)}) %reduce-scatter.5.cloned.1.call-update) | async-done | bytes 1048592 | tf_op jit(solution)/shard_map/reduce_scatter | solution.py:50
  100.7 2.3 copy.51
  103.0 27.9 %reduce-scatter.7.cloned.1.call-done = bf16[128,1024]{1,0:T(8,128)(2,1)} async-done(((bf16[512,1024]{1,0:T(8,128)(2,1)}), bf16[128,1024]{1,0:T(8,128)(2,1)}) %reduce-scatter.7.cloned.1.call-update) | async-done | bytes 262160
  130.9 1.8 copy.52
  133.7 1.8 copy.33
  137.2 1.8 copy.35
  139.0 19.2 %all-gather.15.cloned.1.call-done = bf16[512,1024]{0,1:T(8,128)(2,1)} async-done(((bf16[128,1024]{0,1:T(8,128)(2,1)}), bf16[512,1024]{0,1:T(8,128)(2,1)}) %all-gather.15.cloned.1.call-update) | async-done | bytes 1048592 | tf_op jit(solution)/shard_map/all_gather | solution.py:69
  158.2 2.1 reshape.20
  160.4 2.5 reduce_sum.30
  162.9 2.9 multiply_reduce_fusion
  167.8 2.5 copy.37
  170.3 17.3 %psum.7 = f32[]{:T(128)} all-reduce(f32[]{:T(128)S(6)} %add.28), channel_id=1, replica_groups=mesh['fs'=4,'rep'=4,'tp'=2] {'fs','tp'}, use_global_device_ids=true, to_apply=%region_5.0 | all-reduce | flops 1 | bytes 8 | tf_op jit(solution)/shard_map/psum | solution.py:81
  188.3 7.9 %all-gather.7.cloned.1.call-done = f32[512,512]{0,1:T(8,128)} async-done(((f32[128,512]{0,1:T(8,128)}), f32[512,512]{0,1:T(8,128)}) %all-gather.7.cloned.1.call-update) | async-done | bytes 1048592 | tf_op jit(solution)/shard_map/all_gather | solution.py:84
  196.2 4.2 %fusion.8 = (bf16[512,512]{0,1:T(8,128)(2,1)}, f32[512,512]{0,1:T(8,128)}, f32[512,512]{0,1:T(8,128)}) fusion(f32[512,512]{0,1:T(8,128)} %copy.37, f32[]{:T(128)S(6)} %sqrt.11, f32[512,512]{0,1:T(8,128)} %all-gather.7.cloned.1.call-done, bf16[512,512]{1,0:T(8,128)(2,1)} %param.18), kind=kOutput, calls=%fused_computation.27 | convolution fusion | flops 1611661312 | bytes 5242884 | tf_op jit(solution)/shard_map/dot_general | solution.py:28
  200.7 2.5 copy.39
  203.2 23.2 %all-gather.9.cloned.1.call-done = f32[512,512]{0,1:T(8,128)} async-done(((f32[128,512]{0,1:T(8,128)}), f32[512,512]{0,1:T(8,128)}) %all-gather.9.cloned.1.call-update) | async-done | bytes 1048592 | tf_op jit(solution)/shard_map/all_gather | solution.py:85
  226.5 4.3 %fusion.7 = (bf16[512,512]{0,1:T(8,128)(2,1)}, f32[512,512]{0,1:T(8,128)}, f32[512,512]{0,1:T(8,128)}) fusion(f32[512,512]{0,1:T(8,128)} %copy.39, f32[]{:T(128)S(6)} %sqrt.11, f32[512,512]{0,1:T(8,128)} %all-gather.9.cloned.1.call-done, bf16[512,512]{1,0:T(8,128)(2,1)} %param.19), kind=kOutput, calls=%fused_computation.26 | convolution fusion | flops 1611661312 | bytes 5242884 | tf_op jit(solution)/shard_map/dot_general | solution.py:28
  230.8 1.8 copy.47
  232.6 1.8 copy.46
  234.4 1.8 copy.45
  237.0 2.5 copy.41
  239.5 2.5 copy.43
  242.0 2.5 copy.40
  244.6 2.5 copy.42
  247.1 25.3 %all-gather.11.cloned.1.call-done = bf16[2048,512]{0,1:T(8,128)(2,1)} async-done(((bf16[512,512]{0,1:T(8,128)(2,1)}), bf16[2048,512]{0,1:T(8,128)(2,1)}) %all-gather.11.cloned.1.call-update) | async-done | bytes 2097168 | tf_op jit(solution)/shard_map/all_gather | solution.py:91
  272.4 3.9 %copy.48 = bf16[2048,512]{1,0:T(8,128)(2,1)} copy(bf16[2048,512]{0,1:T(8,128)(2,1)} %all-gather.11.cloned.1.call-done) | data formatting | bytes 4194304
  276.4 42.1 %all-gather.13.cloned.1.call-done = bf16[512,2048]{0,1:T(8,128)(2,1)} async-done(((bf16[512,512]{0,1:T(8,128)(2,1)}), bf16[512,2048]{0,1:T(8,128)(2,1)}) %all-gather.13.cloned.1.call-update) | async-done | bytes 2097168 | tf_op jit(solution)/shard_map/all_gather | solution.py:92
  318.5 3.9 %copy.49 = bf16[512,2048]{1,0:T(8,128)(2,1)} copy(bf16[512,2048]{0,1:T(8,128)(2,1)} %all-gather.13.cloned.1.call-done) | data formatting | bytes 4194304
  (28 shorter events, 8.9 us)
Async XLA Ops:
  7.2 1.9 copy-start
  7.2 89.2 %reduce-scatter.5.cloned.1.call-start = ((), (), s32[]{:S(2)}) async-start(), calls=%async_computation.2 | async-start | bytes 5242880 | tf_op jit(solution)/shard_map/reduce_scatter | solution.py:50
  9.1 3.1 copy-start.2
  9.1 3.1 copy-start.3
  16.7 114.2 %reduce-scatter.7.cloned.1.call-start = ((), (), s32[]{:S(2)}) async-start(), calls=%async_computation.8 | async-start | bytes 1310720
  99.7 33.2 %copy-start.1 = (f32[128,512]{1,0:T(8,128)S(1)}, f32[128,512]{1,0:T(8,128)}, u32[]{:S(2)}) copy-start(f32[128,512]{1,0:T(8,128)} %param.20) | copy-start | bytes 786436
  103.0 55.2 %all-gather.15.cloned.1.call-start = ((), (), s32[]{:S(2)}) async-start(), calls=%async_computation.7 | async-start | bytes 1310720 | tf_op jit(solution)/shard_map/all_gather | solution.py:69
  132.8 63.5 %all-gather.7.cloned.1.call-start = ((), (), s32[]{:S(2)}) async-start(), calls=%async_computation.3 | async-start | bytes 1310720 | tf_op jit(solution)/shard_map/all_gather | solution.py:84
  165.8 60.6 %all-gather.9.cloned.1.call-start = ((), (), s32[]{:S(2)}) async-start(), calls=%async_computation.4 | async-start | bytes 1310720 | tf_op jit(solution)/shard_map/all_gather | solution.py:85
  166.4 106.0 %all-gather.11.cloned.1.call-start = ((), (), s32[]{:S(2)}) async-start(), calls=%async_computation.5 | async-start | bytes 2621440 | tf_op jit(solution)/shard_map/all_gather | solution.py:91
  200.5 118.0 %all-gather.13.cloned.1.call-start = ((), (), s32[]{:S(2)}) async-start(), calls=%async_computation.6 | async-start | bytes 2621440 | tf_op jit(solution)/shard_map/all_gather | solution.py:92
Sparse Core Ops, SparseCore 0:
  16.8 79.5 reduce-scatter.4
  103.1 27.7 reduce-scatter.6
  133.3 24.8 all-gather.14
  166.0 30.2 all-gather.6
  198.2 28.2 all-gather.8
  228.5 43.9 all-gather.10
  274.0 44.4 all-gather.12
